TPU v7x, 32 devices: a whole 2x2x4 slice. The times are simulated.
32 devices in a mesh: sp: 16 (over z, y, x), tp: 2 (over core).
Axes of the slice: x: 2, y: 2, z: 4, core: 2. Of those that a mesh axis runs over, the one named last changes fastest.
Arguments:
- queries: bfloat16 [4096, 1024], P('sp', 'tp'), may hold values from -6 to 6
- keys: bfloat16 [4096, 256], P('sp'), may hold values from -6 to 6
- values: bfloat16 [4096, 256], P('sp'), may hold values from -6 to 6
- query_gain: float32 [128], replicated, may hold values from 1.4 to 5.5
- key_gain: float32 [128], replicated, may hold values from 1.4 to 5.5
- residual_in: bfloat16 [4096, 2048], P(('sp', 'tp')), may hold values from -6 to 6
- out_weight: bfloat16 [1024, 2048], P('tp'), may hold values from -0.1875 to 0.1875
- norm_gain: float32 [2048], replicated, may hold values from 0.1 to 1.9
- gate_weight: bfloat16 [2048, 3072], P('sp', 'tp'), may hold values from -0.125 to 0.125
- up_weight: bfloat16 [2048, 3072], P('sp', 'tp'), may hold values from -0.125 to 0.125
- down_weight: bfloat16 [3072, 2048], P('tp', 'sp'), may hold values from -0.109375 to 0.109375
Outputs:
- result: bfloat16 [4096, 2048], P(('sp', 'tp'))
All inputs are finite; a program needn't handle non-finite values.
Results may differ from a plain program's by a relative error of at most 0.017.
Values may be sent and summed in bfloat16 or wider, within the bound.
A program may use at most 64 MiB of HBM per device.

v0:
```python
import math
import jax
import jax.numpy as jnp
from jax import lax
from jax.sharding import PartitionSpec as P

Q_HEADS = 8
KV_HEADS = 2
GRID_WIDTH = 64
EPS = 1e-06
ROPE_BASE = 10000.0


def normalize(wide_values, gain):
    wide = wide_values.astype(jnp.float32)
    return wide * lax.rsqrt(jnp.mean(wide * wide, axis=-1, keepdims=True) + EPS) * gain


def rotate_pair(segment, angles):
    half_size = segment.shape[-1] // 2
    first = segment[..., :half_size]
    second = segment[..., half_size:]
    cosine = jnp.cos(angles)[:, None, :]
    sine_part = jnp.sin(angles)[:, None, :]
    return jnp.concatenate(
        [first * cosine - second * sine_part, second * cosine + first * sine_part], axis=-1
    )


def grid_rotary(head_rows, positions):
    head_size = head_rows.shape[-1]
    half_size = head_size // 2
    quarter = head_size // 4
    inverse = ROPE_BASE ** (-jnp.arange(quarter, dtype=jnp.float32) * 2.0 / half_size)
    row_angles = (positions // GRID_WIDTH).astype(jnp.float32)[:, None] * inverse
    col_angles = (positions % GRID_WIDTH).astype(jnp.float32)[:, None] * inverse
    return jnp.concatenate(
        [
            rotate_pair(head_rows[..., :half_size], row_angles),
            rotate_pair(head_rows[..., half_size:], col_angles),
        ],
        axis=-1,
    )


def gated(gate_part, lifted):
    return (jax.nn.silu(gate_part) * lifted).astype(jnp.bfloat16)


def local(
    queries,
    keys,
    values,
    query_gain,
    key_gain,
    residual_in,
    out_weight,
    norm_gain,
    gate_weight,
    up_weight,
    down_weight,
):
    tok_rows = queries.shape[0]
    head_size = query_gain.shape[0]
    local_heads = queries.shape[1] // head_size
    tp_index = lax.axis_index("tp")
    share = tok_rows // lax.axis_size("tp")
    positions = lax.axis_index("sp") * tok_rows + jnp.arange(tok_rows, dtype=jnp.int32)
    key_head = tp_index * local_heads // (Q_HEADS // KV_HEADS)
    own_keys = lax.dynamic_slice_in_dim(keys, key_head * head_size, head_size, 1)
    own_values = lax.dynamic_slice_in_dim(values, key_head * head_size, head_size, 1)
    turned_keys = grid_rotary(
        normalize(own_keys.reshape(tok_rows, 1, head_size), key_gain), positions
    )
    turned_keys = turned_keys.reshape(tok_rows, head_size).astype(jnp.bfloat16)
    turned_queries = grid_rotary(
        normalize(queries.reshape(tok_rows, local_heads, head_size), query_gain), positions
    )
    turned_queries = turned_queries.reshape(tok_rows * local_heads, head_size).astype(jnp.bfloat16)
    score_scale = head_size ** (-0.5)

    def attend_block(running, block_pair):
        peak_score, weight_total, weighted = running
        block_keys, block_values = block_pair
        scores = (
            lax.dot_general(
                turned_queries,
                block_keys,
                (((1,), (1,)), ((), ())),
                preferred_element_type=jnp.float32,
            )
            * score_scale
        )
        new_peak = jnp.maximum(peak_score, jnp.max(scores, axis=1))
        factor = jnp.exp(peak_score - new_peak)
        raw = jnp.exp(scores - new_peak[:, None])
        weight_total = weight_total * factor + jnp.sum(raw, axis=1)
        weighted = weighted * factor[:, None] + jnp.dot(
            raw.astype(jnp.bfloat16), block_values, preferred_element_type=jnp.float32
        )
        return ((new_peak, weight_total, weighted), None)

    row_count = tok_rows * local_heads
    start_carry = (
        jnp.full((row_count,), -1e30, jnp.float32),
        jnp.zeros((row_count,), jnp.float32),
        jnp.zeros((row_count, head_size), jnp.float32),
    )
    piece_keys = lax.all_gather(turned_keys, "sp", axis=0, tiled=True)
    piece_values = lax.all_gather(own_values, "sp", axis=0, tiled=True)
    span = math.gcd(piece_keys.shape[0], 512)
    blocks = piece_keys.shape[0] // span
    stacked = (
        piece_keys.reshape(blocks, span, head_size),
        piece_values.reshape(blocks, span, head_size),
    )
    updated, unused = lax.scan(attend_block, start_carry, stacked)
    peak_score, weight_total, weighted = updated
    attended = (
        (weighted / weight_total[:, None])
        .astype(jnp.bfloat16)
        .reshape(tok_rows, local_heads * head_size)
    )
    placed = lax.dynamic_update_slice_in_dim(
        jnp.zeros((tok_rows, residual_in.shape[1]), jnp.float32),
        residual_in.astype(jnp.float32),
        tp_index * share,
        0,
    )
    head_partial = jnp.dot(attended, out_weight, preferred_element_type=jnp.float32)
    partial_total, residual_rows = (
        lax.psum(head_partial.astype(jnp.bfloat16), "tp").astype(jnp.float32),
        lax.psum(placed.astype(jnp.bfloat16), "tp").astype(jnp.float32),
    )
    middle_rows = (residual_rows + partial_total).astype(jnp.bfloat16)
    normed = normalize(middle_rows, norm_gain).astype(jnp.bfloat16)
    middle = lax.dynamic_slice_in_dim(middle_rows, tp_index * share, share, 0)
    hidden_width = gate_weight.shape[1]
    side_by_side = jnp.concatenate(
        [
            lax.all_gather(gate_weight, "sp", axis=0, tiled=True),
            lax.all_gather(up_weight, "sp", axis=0, tiled=True),
        ],
        axis=1,
    )
    both_parts = jnp.dot(normed, side_by_side, preferred_element_type=jnp.float32)
    hidden = gated(both_parts[:, :hidden_width], both_parts[:, hidden_width:])
    partials = jnp.dot(
        hidden,
        lax.all_gather(down_weight, "sp", axis=1, tiled=True),
        preferred_element_type=jnp.float32,
    )
    mixer_out = lax.psum_scatter(
        partials.astype(jnp.bfloat16), "tp", scatter_dimension=0, tiled=True
    ).astype(jnp.float32)
    return (middle.astype(jnp.float32) + mixer_out).astype(jnp.bfloat16)


def solution(mesh):
    return jax.shard_map(
        local,
        mesh=mesh,
        in_specs=(
            P("sp", "tp"),
            P("sp", None),
            P("sp", None),
            P(),
            P(),
            P(("sp", "tp"), None),
            P("tp", None),
            P(),
            P("sp", "tp"),
            P("sp", "tp"),
            P("tp", "sp"),
        ),
        out_specs=P(("sp", "tp"), None),
        check_vma=False,
    )
```

profile of v0, /device:TPU:0, one launch (start us, length us, event | category | flops | bytes accessed | tf_op | source)
XLA Modules:
  0.0 528.7 jit_solution(11063251506600256293)
XLA Ops:
  17.7 50.1 %all-gather.15.cloned.1.call-done = bf16[4096,1,128]{0,2,1:T(8,128)(2,1)} async-done(((bf16[256,1,128]{0,2,1:T(8,128)(2,1)}), bf16[4096,1,128]{0,2,1:T(8,128)(2,1)}) %all-gather.15.cloned.1.call-update) | async-done | bytes 1048592 | tf_op jit(solution)/shard_map/all_gather | solution.py:109
  67.8 2.3 copy.19
  70.1 54.3 %all-gather.7.cloned.1.call-done = bf16[4096,128]{1,0:T(8,128)(2,1)} async-done(((bf16[256,128]{1,0:T(8,128)(2,1)}), bf16[4096,128]{1,0:T(8,128)(2,1)}) %all-gather.7.cloned.1.call-update) | async-done | bytes 1048592 | tf_op jit(solution)/shard_map/all_gather | solution.py:110
  124.4 51.7 %while.15 = (s32[]{:T(128)}, f32[1024]{0:T(1024)S(1)}, f32[1024]{0:T(1024)S(1)}, f32[1024,128]{1,0:T(8,128)S(1)}, bf16[8,512,128]{2,1,0:T(8,128)(2,1)}, /*index=...) while((s32[]{:T(128)}, f32[1024]{0:T(1024)S(1)}, ...), condition=%wide.region_6.7_spmd.clone, body=%wide.region_3.6_spmd.clone.sunk | while | flops 273028096 | bytes 16319621 | solution.py:117
  124.4 2.7 multiply_reduce_fusion.3
  127.0 2.1 fusion.63
  130.8 2.7 multiply_reduce_fusion.3
  133.5 2.1 fusion.63
  137.3 2.7 multiply_reduce_fusion.3
  140.0 2.1 fusion.63
  143.7 2.7 multiply_reduce_fusion.3
  146.4 2.1 fusion.63
  148.6 1.5 convolution_add_fusion.2
  150.2 2.7 multiply_reduce_fusion.3
  152.9 2.1 fusion.63
  156.7 2.7 multiply_reduce_fusion.3
  159.3 2.1 fusion.63
  163.1 2.7 multiply_reduce_fusion.3
  165.8 2.1 fusion.63
  168.0 1.5 convolution_add_fusion.2
  169.6 2.7 multiply_reduce_fusion.3
  172.3 2.1 fusion.63
  176.4 1.7 convolution_convert_fusion
  179.9 18.6 %all-reduce.3.cloned.1.call-done = (bf16[256,2048]{1,0:T(8,128)(2,1)}, bf16[256,2048]{1,0:T(8,128)(2,1)}) async-done(((bf16[256,2048]{1,0:T(8,128)(2,1)}, bf16[256,2048]{1,0:T(8,128)(2,1)}), (bf16[256,2048]{1,0:T(8,128)(2,1)}, bf16[256,2048]{1,0:T(8,128)(2,1)})) %all-reduce.3.cloned.1.call-update) | async-done | bytes 2097168 | tf_op jit(solution)/shard_map/psum | solution.py:132
  198.5 2.0 fusion.18
  200.6 95.2 %all-gather.11.cloned.1.call-done = bf16[2048,1536]{1,0:T(8,128)(2,1)} async-done(((bf16[128,1536]{1,0:T(8,128)(2,1)}), bf16[2048,1536]{1,0:T(8,128)(2,1)}) %all-gather.11.cloned.1.call-update) | async-done | bytes 6291472 | tf_op jit(solution)/shard_map/all_gather | solution.py:142
  295.8 94.6 %all-gather.9.cloned.1.call-done = bf16[2048,1536]{1,0:T(8,128)(2,1)} async-done(((bf16[128,1536]{1,0:T(8,128)(2,1)}), bf16[2048,1536]{1,0:T(8,128)(2,1)}) %all-gather.9.cloned.1.call-update) | async-done | bytes 6291472 | tf_op jit(solution)/shard_map/all_gather | solution.py:141
  390.4 9.8 %fusion.14 = f32[256,3072]{1,0:T(8,128)} fusion(bf16[2048,1536]{1,0:T(8,128)(2,1)} %all-gather.11.cloned.1.call-done, bf16[2048,1536]{1,0:T(8,128)(2,1)} %all-gather.9.cloned.1.call-done, bf16[256,2048]{1,0:T(8,128)(2,1)S(1)} %get-tuple-element.102, f32[2048]{0:T(1024)S(1)} %copy-done.4, f32[256]{0:T(256)S(1)} %add_rsqrt_fusion.1), kind=kOutput, calls=%fused_computation.20 | convolution fusion | flops 3248488448 | bytes 16786432 | tf_op jit(solution)/shard_map/dot_general | solution.py:146
  400.2 106.3 %all-gather.13.cloned.1.call-done = bf16[1536,2048]{1,0:T(8,128)(2,1)} async-done(((bf16[1536,128]{1,0:T(8,128)(2,1)}), bf16[1536,2048]{1,0:T(8,128)(2,1)}) %all-gather.13.cloned.1.call-update) | async-done | bytes 6291472 | tf_op jit(solution)/shard_map/all_gather | solution.py:150
  506.5 6.6 %convolution_convert_fusion.1 = bf16[256,2048]{1,0:T(8,128)(2,1)} fusion(bf16[1536,2048]{1,0:T(8,128)(2,1)} %all-gather.13.cloned.1.call-done, f32[256,3072]{1,0:T(8,128)} %fusion.14), kind=kOutput, calls=%fused_computation.27 | convolution fusion | flops 1613496320 | bytes 10485760 | tf_op jit(solution)/shard_map/dot_general | solution.py:148
  513.1 6.7 %reduce-scatter.2.cloned.1.call-done = bf16[128,2048]{1,0:T(8,128)(2,1)} async-done(((bf16[256,2048]{1,0:T(8,128)(2,1)}), bf16[128,2048]{1,0:T(8,128)(2,1)}) %reduce-scatter.2.cloned.1.call-update) | async-done | bytes 524304 | tf_op jit(solution)/shard_map/reduce_scatter | solution.py:153
  519.9 2.0 add_convert_fusion.1
  (93 shorter events, 23.2 us)
Async XLA Ops:
  6.5 169.9 %copy-start = (bf16[512,2048]{1,0:T(8,128)(2,1)S(1)}, bf16[512,2048]{1,0:T(8,128)(2,1)}, u32[]{:S(2)}) copy-start(bf16[512,2048]{1,0:T(8,128)(2,1)} %param.19) | copy-start | bytes 6291460
  6.5 7.1 %copy-start.3 = (f32[128]{0:T(128)S(1)}, f32[128]{0:T(128)}, u32[]{:S(2)}) copy-start(f32[128]{0:T(128)} %param.16) | copy-start | bytes 1540
  6.5 61.3 %all-gather.15.cloned.1.call-start = ((), (), s32[]{:S(2)}) async-start(), calls=%async_computation.6 | async-start | bytes 1114112 | tf_op jit(solution)/shard_map/all_gather | solution.py:109
  9.5 114.9 %all-gather.7.cloned.1.call-start = ((), (), s32[]{:S(2)}) async-start(), calls=%async_computation.1 | async-start | bytes 1114112 | tf_op jit(solution)/shard_map/all_gather | solution.py:110
  11.0 187.5 %all-reduce.3.cloned.1.call-start = ((), (), s32[]{:S(2)}) async-start(), calls=%async_computation.7 | async-start | bytes 4194304 | tf_op jit(solution)/shard_map/psum | solution.py:132
  14.8 2.0 copy-start.2
  127.0 2.2 copy-start.1
  133.5 2.2 copy-start.1
  140.0 2.2 copy-start.1
  146.4 2.2 copy-start.1
  152.9 2.2 copy-start.1
  159.3 2.2 copy-start.1
  165.8 2.2 copy-start.1
  172.3 2.2 copy-start.1
  178.1 212.2 %copy-start.4 = (f32[2048]{0:T(1024)S(1)}, f32[2048]{0:T(1024)}, u32[]{:S(2)}) copy-start(f32[2048]{0:T(1024)} %param.20) | copy-start | bytes 24580
  178.1 117.6 %all-gather.11.cloned.1.call-start = ((), (), s32[]{:S(2)}) async-start(), calls=%async_computation.3 | async-start | bytes 6684672 | tf_op jit(solution)/shard_map/all_gather | solution.py:142
  178.7 211.6 %all-gather.9.cloned.1.call-start = ((), (), s32[]{:S(2)}) async-start(), calls=%async_computation.2 | async-start | bytes 6684672 | tf_op jit(solution)/shard_map/all_gather | solution.py:141
  179.3 327.2 %all-gather.13.cloned.1.call-start = ((), (), s32[]{:S(2)}) async-start(), calls=%async_computation.4 | async-start | bytes 6684672 | tf_op jit(solution)/shard_map/all_gather | solution.py:150
  179.9 340.0 %reduce-scatter.2.cloned.1.call-start = ((), (), s32[]{:S(2)}) async-start(), calls=%async_computation.5 | async-start | bytes 1572864 | tf_op jit(solution)/shard_map/reduce_scatter | solution.py:153
Sparse Core Ops, SparseCore 0:
  10.1 57.6 all-gather.14
  70.6 53.7 all-gather.6
  178.3 20.2 all-reduce.2
  201.1 94.5 all-gather.10
  298.4 91.9 all-gather.8
  392.9 113.5 all-gather.12
  513.2 6.5 reduce-scatter.1
where the time goes:
time: 529 us
  waiting for transfers between devices  428 us (81%)
  matrix products  51.7 us (10%)
  other arithmetic  27.3 us (5%)
  between operations  13.7 us (3%)
  local copies, waits for them, and re-layouts  8.01 us (2%)
    all_gather x1, waiting for transfers between devices, local(): lax.all_gather(down_weight, 'sp', axis=1, tiled=True)  106 us
    all_gather x1, waiting for transfers between devices, local(): lax.all_gather(up_weight, 'sp', axis=0, tiled=True)  95.2 us
    all_gather x1, waiting for transfers between devices, local(): lax.all_gather(gate_weight, 'sp', axis=0, tiled=True)  94.6 us
    all_gather x1, waiting for transfers between devices, local(): piece_values = lax.all_gather(own_values, 'sp', axis=0, tiled=True)  54.3 us
    all_gather x1, waiting for transfers between devices, local(): piece_keys = lax.all_gather(turned_keys, 'sp', axis=0, tiled=True)  50.1 us
    dot_general x8, matrix products, attend_block(): lax.dot_general(turned_queries, block_keys, (((1,), (1,)), ((), ())), pre...  21.4 us
    psum x1, waiting for transfers between devices, local(): lax.psum(head_partial.astype(jnp.bfloat16), 'tp').astype(jnp.float32)  18.6 us
    reduce_sum x8, other arithmetic, attend_block(): weight_total = weight_total * factor + jnp.sum(raw, axis=1)  16.9 us
  transfers between devices with their start and end apart: 7, of which 7 were waited for; matrix products, arithmetic and copies ran while one was open for 4% of the time, Pallas kernels for 0%

commit v1 on v0

--- a/solution.py
+++ b/solution.py
@@ -3,12 +3,18 @@
 import jax.numpy as jnp
 from jax import lax
 from jax.sharding import PartitionSpec as P
+from jax.lax import all_gather
 
 Q_HEADS = 8
 KV_HEADS = 2
 GRID_WIDTH = 64
 EPS = 1e-06
 ROPE_BASE = 10000.0
+
+
+def _edit_samples(mesh_ax, pos_dim, own_rows):
+    top = jnp.concatenate(all_gather(own_rows, mesh_ax), pos_dim)
+    return top
 
 
 def normalize(wide_values, gain):
@@ -146,9 +152,7 @@
     both_parts = jnp.dot(normed, side_by_side, preferred_element_type=jnp.float32)
     hidden = gated(both_parts[:, :hidden_width], both_parts[:, hidden_width:])
     partials = jnp.dot(
-        hidden,
-        lax.all_gather(down_weight, "sp", axis=1, tiled=True),
-        preferred_element_type=jnp.float32,
+        hidden, _edit_samples("sp", 1, down_weight), preferred_element_type=jnp.float32
     )
     mixer_out = lax.psum_scatter(
         partials.astype(jnp.bfloat16), "tp", scatter_dimension=0, tiled=True

time: 529 us -> 513 us (0.970)
  waiting for transfers between devices: 428 us -> 407 us
  local copies, waits for them, and re-layouts: 8.01 us -> 16.8 us
  matrix products: 51.7 us -> 46.4 us
    all_gather x1, waiting for transfers between devices: 106 us -> 95.2 us  [_edit_samples(): top = jnp.concatenate(all_gather(own_rows, mesh_ax), pos_dim)]
    all_gather x1, waiting for transfers between devices: 94.6 us -> 85.8 us  [local(): lax.all_gather(gate_weight, 'sp', axis=0, tiled=True)]
    reshape x0 -> x1, local copies, waits for them, and re-layouts: none -> 8.76 us  [_edit_samples(): top = jnp.concatenate(all_gather(own_rows, mesh_ax), pos_dim)]
where the time goes in v1:
time: 513 us; the launch traced here: 512 us
  waiting for transfers between devices  407 us (79%)
  matrix products  46.4 us (9%)
  other arithmetic  27.3 us (5%)
  local copies, waits for them, and re-layouts  16.8 us (3%)
  between operations  13.7 us (3%)
    all_gather x1, waiting for transfers between devices, _edit_samples(): top = jnp.concatenate(all_gather(own_rows, mesh_ax), pos_dim)  95.2 us
    all_gather x1, waiting for transfers between devices, local(): lax.all_gather(up_weight, 'sp', axis=0, tiled=True)  94.6 us
    all_gather x1, waiting for transfers between devices, local(): lax.all_gather(gate_weight, 'sp', axis=0, tiled=True)  85.8 us
    all_gather x1, waiting for transfers between devices, local(): piece_values = lax.all_gather(own_values, 'sp', axis=0, tiled=True)  54.3 us
    all_gather x1, waiting for transfers between devices, local(): piece_keys = lax.all_gather(turned_keys, 'sp', axis=0, tiled=True)  50.1 us
    dot_general x8, matrix products, attend_block(): lax.dot_general(turned_queries, block_keys, (((1,), (1,)), ((), ())), pre...  21.4 us
    psum x1, waiting for transfers between devices, local(): lax.psum(head_partial.astype(jnp.bfloat16), 'tp').astype(jnp.float32)  18.4 us
    reduce_sum x8, other arithmetic, attend_block(): weight_total = weight_total * factor + jnp.sum(raw, axis=1)  16.9 us
  transfers between devices with their start and end apart: 7, of which 7 were waited for; matrix products, arithmetic and copies ran while one was open for 4% of the time, Pallas kernels for 0%

profile of v1, /device:TPU:0, one launch (start us, length us, event | category | flops | bytes accessed | tf_op | source)
XLA Modules:
  0.0 511.9 jit_solution(1291841046959933060)
XLA Ops:
  17.7 50.1 %all-gather.14.cloned.1.call-done = bf16[4096,1,128]{0,2,1:T(8,128)(2,1)} async-done(((bf16[256,1,128]{0,2,1:T(8,128)(2,1)}), bf16[4096,1,128]{0,2,1:T(8,128)(2,1)}) %all-gather.14.cloned.1.call-update) | async-done | bytes 1048592 | tf_op jit(solution)/shard_map/all_gather | solution.py:115
  67.8 2.3 copy.22
  70.1 54.3 %all-gather.8.cloned.1.call-done = bf16[4096,128]{1,0:T(8,128)(2,1)} async-done(((bf16[256,128]{1,0:T(8,128)(2,1)}), bf16[4096,128]{1,0:T(8,128)(2,1)}) %all-gather.8.cloned.1.call-update) | async-done | bytes 1048592 | tf_op jit(solution)/shard_map/all_gather | solution.py:116
  124.4 51.6 %while.15 = (s32[]{:T(128)}, f32[1024]{0:T(1024)S(1)}, f32[1024]{0:T(1024)S(1)}, f32[1024,128]{1,0:T(8,128)S(1)}, bf16[8,512,128]{2,1,0:T(8,128)(2,1)}, /*index=...) while((s32[]{:T(128)}, f32[1024]{0:T(1024)S(1)}, ...), condition=%wide.region_6.7_spmd.clone, body=%wide.region_3.6_spmd.clone.sunk | while | flops 273028096 | bytes 16319621 | solution.py:123
  124.4 2.7 multiply_reduce_fusion.3
  127.0 2.1 fusion.63
  130.8 2.7 multiply_reduce_fusion.3
  133.5 2.1 fusion.63
  137.3 2.7 multiply_reduce_fusion.3
  140.0 2.1 fusion.63
  142.2 1.5 convolution_add_fusion.2
  143.7 2.7 multiply_reduce_fusion.3
  146.4 2.1 fusion.63
  150.2 2.7 multiply_reduce_fusion.3
  152.9 2.1 fusion.63
  156.6 2.7 multiply_reduce_fusion.3
  159.3 2.1 fusion.63
  163.1 2.7 multiply_reduce_fusion.3
  165.8 2.1 fusion.63
  169.5 2.7 multiply_reduce_fusion.3
  172.2 2.1 fusion.63
  176.4 1.7 convolution_convert_fusion
  180.1 18.4 %all-reduce.3.cloned.1.call-done = (bf16[256,2048]{1,0:T(8,128)(2,1)}, bf16[256,2048]{1,0:T(8,128)(2,1)}) async-done(((bf16[256,2048]{1,0:T(8,128)(2,1)}, bf16[256,2048]{1,0:T(8,128)(2,1)}), (bf16[256,2048]{1,0:T(8,128)(2,1)}, bf16[256,2048]{1,0:T(8,128)(2,1)})) %all-reduce.3.cloned.1.call-update) | async-done | bytes 2097168 | tf_op jit(solution)/shard_map/psum | solution.py:138
  198.5 2.0 fusion.18
  200.6 95.2 %all-gather.16.cloned.1.call-done = bf16[24576,128]{1,0:T(8,128)(2,1)} async-done(((bf16[1536,128]{1,0:T(8,128)(2,1)}), bf16[24576,128]{1,0:T(8,128)(2,1)}) %all-gather.16.cloned.1.call-update) | async-done | bytes 6291472 | tf_op jit(solution)/shard_map/all_gather | solution.py:16
  295.7 8.8 %copy.21 = bf16[1536,16,128]{0,2,1:T(8,128)(2,1)} copy(bf16[1536,16,128]{2,0,1:T(8,128)(2,1)} %bitcast.28) | data formatting | bytes 12582912 | tf_op jit(solution)/shard_map/reshape | solution.py:16
  304.5 85.8 %all-gather.10.cloned.1.call-done = bf16[2048,1536]{1,0:T(8,128)(2,1)} async-done(((bf16[128,1536]{1,0:T(8,128)(2,1)}), bf16[2048,1536]{1,0:T(8,128)(2,1)}) %all-gather.10.cloned.1.call-update) | async-done | bytes 6291472 | tf_op jit(solution)/shard_map/all_gather | solution.py:147
  390.3 94.6 %all-gather.12.cloned.1.call-done = bf16[2048,1536]{1,0:T(8,128)(2,1)} async-done(((bf16[128,1536]{1,0:T(8,128)(2,1)}), bf16[2048,1536]{1,0:T(8,128)(2,1)}) %all-gather.12.cloned.1.call-update) | async-done | bytes 6291472 | tf_op jit(solution)/shard_map/all_gather | solution.py:148
  484.9 8.3 %fusion.14 = f32[256,3072]{1,0:T(8,128)S(1)} fusion(bf16[2048,1536]{1,0:T(8,128)(2,1)} %all-gather.12.cloned.1.call-done, bf16[2048,1536]{1,0:T(8,128)(2,1)} %all-gather.10.cloned.1.call-done, bf16[256,2048]{1,0:T(8,128)(2,1)S(1)} %get-tuple-element.102, f32[2048]{0:T(1024)S(1)} %copy-done.5, f32[256]{0:T(256)S(1)} %add_rsqrt_fusion.1), kind=kOutput, calls=%fused_computation.20 | convolution fusion | flops 3248488448 | bytes 16786432 | tf_op jit(solution)/shard_map/dot_general | solution.py:152
  493.2 2.8 convolution_convert_fusion.1
  496.0 7.1 %reduce-scatter.2.cloned.1.call-done = bf16[128,2048]{1,0:T(8,128)(2,1)} async-done(((bf16[256,2048]{1,0:T(8,128)(2,1)}), bf16[128,2048]{1,0:T(8,128)(2,1)}) %reduce-scatter.2.cloned.1.call-update) | async-done | bytes 524304 | tf_op jit(solution)/shard_map/reduce_scatter | solution.py:157
  503.1 2.0 add_convert_fusion.1
  (96 shorter events, 24.9 us)
Async XLA Ops:
  6.5 169.8 %copy-start = (bf16[512,2048]{1,0:T(8,128)(2,1)S(1)}, bf16[512,2048]{1,0:T(8,128)(2,1)}, u32[]{:S(2)}) copy-start(bf16[512,2048]{1,0:T(8,128)(2,1)} %param.19) | copy-start | bytes 6291460
  6.5 7.1 %copy-start.4 = (f32[128]{0:T(128)S(1)}, f32[128]{0:T(128)}, u32[]{:S(2)}) copy-start(f32[128]{0:T(128)} %param.16) | copy-start | bytes 1540
  6.5 61.3 %all-gather.14.cloned.1.call-start = ((), (), s32[]{:S(2)}) async-start(), calls=%async_computation.5 | async-start | bytes 1114112 | tf_op jit(solution)/shard_map/all_gather | solution.py:115
  9.5 114.9 %all-gather.8.cloned.1.call-start = ((), (), s32[]{:S(2)}) async-start(), calls=%async_computation.1 | async-start | bytes 1114112 | tf_op jit(solution)/shard_map/all_gather | solution.py:116
  11.0 187.5 %all-reduce.3.cloned.1.call-start = ((), (), s32[]{:S(2)}) async-start(), calls=%async_computation.7 | async-start | bytes 4194304 | tf_op jit(solution)/shard_map/psum | solution.py:138
  14.9 2.0 copy-start.3
  127.0 2.2 copy-start.1
  133.5 2.2 copy-start.1
  139.9 2.2 copy-start.1
  146.4 2.2 copy-start.1
  152.9 2.2 copy-start.1
  159.3 2.2 copy-start.1
  165.8 2.2 copy-start.1
  172.2 2.2 copy-start.1
  178.1 117.6 %all-gather.16.cloned.1.call-start = ((), (), s32[]{:S(2)}) async-start(), calls=%async_computation.6 | async-start | bytes 6684672 | tf_op jit(solution)/shard_map/all_gather | solution.py:16
  178.7 211.6 %all-gather.10.cloned.1.call-start = ((), (), s32[]{:S(2)}) async-start(), calls=%async_computation.2 | async-start | bytes 6684672 | tf_op jit(solution)/shard_map/all_gather | solution.py:147
  179.3 305.6 %all-gather.12.cloned.1.call-start = ((), (), s32[]{:S(2)}) async-start(), calls=%async_computation.3 | async-start | bytes 6684672 | tf_op jit(solution)/shard_map/all_gather | solution.py:148
  179.9 323.3 %reduce-scatter.2.cloned.1.call-start = ((), (), s32[]{:S(2)}) async-start(), calls=%async_computation.4 | async-start | bytes 1572864 | tf_op jit(solution)/shard_map/reduce_scatter | solution.py:157
  295.7 189.2 %copy-start.5 = (f32[2048]{0:T(1024)S(1)}, f32[2048]{0:T(1024)}, u32[]{:S(2)}) copy-start(f32[2048]{0:T(1024)} %param.20) | copy-start | bytes 24580
  484.9 8.3 %copy-start.2 = (bf16[1536,16,128]{0,2,1:T(8,128)(2,1)S(1)}, bf16[1536,16,128]{0,2,1:T(8,128)(2,1)}, u32[]{:S(2)}) copy-start(bf16[1536,16,128]{0,2,1:T(8,128)(2,1)} %copy.21) | copy-start | bytes 18874372
Sparse Core Ops, SparseCore 0:
  10.1 57.6 all-gather.13
  70.6 53.7 all-gather.7
  178.2 20.2 all-reduce.2
  201.1 94.5 all-gather.15
  298.4 91.9 all-gather.9
  393.0 91.9 all-gather.11
  496.2 6.8 reduce-scatter.1
